TPU v7x, 32 devices: a whole 2x2x4 slice. The times are simulated.
32 devices in a mesh: ep: 8 (over z, y), tp: 4 (over x, core).
Axes of the slice: x: 2, y: 2, z: 4, core: 2. Of those that a mesh axis runs over, the one named last changes fastest.
Arguments:
- tokens: bfloat16 [1024, 2048], P('ep'), may hold values from -6 to 6
- cotangent: bfloat16 [1024, 2048], P('ep'), may hold values from -2 to 2
- route_weights: float32 [1024, 2], P('ep'), may hold values from 0.25 to 2.5
- routes: int32 [1024, 2], P('ep'), may hold values from 0 to 7, all different within a row; in each aligned block of 128 rows (0 to 127, 128 to 255, ...) at most 64 rows name the same one
- gate_proj: bfloat16 [8, 2048, 512], P('ep', None, 'tp'), may hold values from -0.125 to 0.125
- up_proj: bfloat16 [8, 2048, 512], P('ep', None, 'tp'), may hold values from -0.125 to 0.125
- down_proj: bfloat16 [8, 512, 2048], P('ep', 'tp'), may hold values from -0.25 to 0.25
- shared_down: bfloat16 [2048, 512], P(None, 'tp'), may hold values from -0.25 to 0.25
- shared_hidden: bfloat16 [1024, 512], P('ep', 'tp'), may hold values from -0.29882812 to 0.29882812
Outputs:
- tokens_grad: bfloat16 [1024, 2048], P('ep', 'tp')
- weights_grad: float32 [1024, 2], P('ep')
- gate_proj_grad: bfloat16 [8, 2048, 512], P('ep', None, 'tp')
- up_proj_grad: bfloat16 [8, 2048, 512], P('ep', None, 'tp')
- down_proj_grad: bfloat16 [8, 512, 2048], P('ep', 'tp')
- hidden_grad: bfloat16 [1024, 512], P('ep', 'tp')
- shared_grad: float32 [2048, 512], P('ep', 'tp')
Inputs may be any that keep to these rules, and one draw needn't show every extreme that they name: `routes`: in each aligned block of 128 rows no expert is named more than 64 times, a bound that some block reaches; the 2 experts of a row differ.
All inputs are finite; a program needn't handle non-finite values.
Results may differ from a plain program's by a relative error of at most 0.012.
Values may be sent and summed in bfloat16 or wider, within the bound.
A program may use at most 64 MiB of HBM per device.

v0:
```python
import jax
import jax.numpy as jnp
from jax import lax
from jax.sharding import PartitionSpec as P


def shards(
    tokens,
    cotangent,
    route_weights,
    routes,
    gate_proj,
    up_proj,
    down_proj,
    shared_down,
    shared_hidden,
):
    tok_rows, feat_width = tokens.shape
    top_count = routes.shape[1]
    exp_local = gate_proj.shape[0]
    ep_size = lax.axis_size("ep")
    tp_size = lax.axis_size("tp")
    exp_total = exp_local * ep_size
    capacity = 2 * tok_rows * top_count // exp_total
    quarter = feat_width // tp_size
    filled = exp_total * capacity
    flat_routes = routes.reshape(-1)
    one_hot = (flat_routes[:, None] == jnp.arange(exp_total, dtype=jnp.int32)[None, :]).astype(
        jnp.int32
    )
    rank_in = jnp.sum((jnp.cumsum(one_hot, axis=0) - one_hot) * one_hot, axis=1)
    slot_ids = flat_routes * capacity + rank_in
    route_owner = jnp.arange(flat_routes.shape[0], dtype=jnp.int32) // top_count
    owner_ids = jnp.full((filled,), tok_rows, jnp.int32).at[slot_ids].set(route_owner)
    sent_weights = (
        jnp.zeros((filled,), jnp.bfloat16)
        .at[slot_ids]
        .set(route_weights.reshape(-1).astype(jnp.bfloat16))
    )
    first_col = lax.axis_index("tp") * quarter
    own_rows = lax.dynamic_slice_in_dim(tokens, first_col, quarter, 1)
    own_grads = lax.dynamic_slice_in_dim(cotangent, first_col, quarter, 1)
    sent_rows = jnp.take(own_rows, owner_ids, axis=0, mode="fill", fill_value=0)
    sent_grads = jnp.take(own_grads, owner_ids, axis=0, mode="fill", fill_value=0)
    got_rows, got_grads, got_weights = (
        lax.all_to_all(sent_rows, "ep", split_axis=0, concat_axis=0, tiled=True),
        lax.all_to_all(sent_grads, "ep", split_axis=0, concat_axis=0, tiled=True),
        lax.all_to_all(sent_weights, "ep", split_axis=0, concat_axis=0, tiled=True),
    )
    got_rows, got_grads = (
        lax.all_gather(got_rows, "tp", axis=1, tiled=True),
        lax.all_gather(got_grads, "tp", axis=1, tiled=True),
    )
    slot_rows = got_rows.reshape(ep_size, exp_local, capacity, feat_width)
    slot_grads = got_grads.reshape(ep_size, exp_local, capacity, feat_width)
    weight_col = got_weights.reshape(ep_size, exp_local, capacity, 1).astype(jnp.float32)
    gate = jnp.einsum("secd,edf->secf", slot_rows, gate_proj, preferred_element_type=jnp.float32)
    upper = jnp.einsum("secd,edf->secf", slot_rows, up_proj, preferred_element_type=jnp.float32)
    active = jax.nn.silu(gate)
    hidden = (active * upper).astype(jnp.bfloat16)
    backed = jnp.einsum("secd,efd->secf", slot_grads, down_proj, preferred_element_type=jnp.float32)
    gate_share = jnp.sum(hidden.astype(jnp.float32) * backed, axis=3)
    d_hidden = weight_col * backed
    sigma = jax.nn.sigmoid(gate)
    d_gate = (d_hidden * upper * sigma * (1.0 + gate * (1.0 - sigma))).astype(jnp.bfloat16)
    d_up = (d_hidden * active).astype(jnp.bfloat16)
    scaled = (weight_col * slot_grads).astype(jnp.bfloat16)
    down_proj_grad = jnp.einsum(
        "secf,secd->efd", hidden, scaled, preferred_element_type=jnp.float32
    ).astype(jnp.bfloat16)
    gate_proj_grad = jnp.einsum(
        "secd,secf->edf", slot_rows, d_gate, preferred_element_type=jnp.float32
    ).astype(jnp.bfloat16)
    up_proj_grad = jnp.einsum(
        "secd,secf->edf", slot_rows, d_up, preferred_element_type=jnp.float32
    ).astype(jnp.bfloat16)
    partial_value = jnp.einsum(
        "secf,edf->secd", d_gate, gate_proj, preferred_element_type=jnp.float32
    )
    partial_value = partial_value + jnp.einsum(
        "secf,edf->secd", d_up, up_proj, preferred_element_type=jnp.float32
    )
    gate_whole = lax.psum(gate_share, "tp")
    input_cols = lax.psum_scatter(
        partial_value.astype(jnp.bfloat16), "tp", scatter_dimension=3, tiled=True
    )
    back_cols, back_gate = (
        lax.all_to_all(
            input_cols.reshape(filled, quarter), "ep", split_axis=0, concat_axis=0, tiled=True
        ),
        lax.all_to_all(
            gate_whole.astype(jnp.bfloat16).reshape(filled),
            "ep",
            split_axis=0,
            concat_axis=0,
            tiled=True,
        ),
    )
    picked = back_cols[slot_ids].reshape(tok_rows, top_count, quarter)
    tokens_grad = jnp.sum(picked.astype(jnp.float32), axis=1).astype(jnp.bfloat16)
    weights_grad = back_gate[slot_ids].astype(jnp.float32).reshape(tok_rows, top_count)
    hidden_grad = jnp.dot(cotangent, shared_down, preferred_element_type=jnp.float32).astype(
        jnp.bfloat16
    )
    shared_grad = lax.psum_scatter(
        jnp.einsum("td,th->dh", cotangent, shared_hidden, preferred_element_type=jnp.float32),
        "ep",
        scatter_dimension=0,
        tiled=True,
    )
    return (
        tokens_grad,
        weights_grad,
        gate_proj_grad,
        up_proj_grad,
        down_proj_grad,
        hidden_grad,
        shared_grad,
    )


def solution(mesh):
    in_specs = (
        P("ep", None),
        P("ep", None),
        P("ep", None),
        P("ep", None),
        P("ep", None, "tp"),
        P("ep", None, "tp"),
        P("ep", "tp", None),
        P(None, "tp"),
        P("ep", "tp"),
    )
    out_specs = (
        P("ep", "tp"),
        P("ep", None),
        P("ep", None, "tp"),
        P("ep", None, "tp"),
        P("ep", "tp", None),
        P("ep", "tp"),
        P("ep", "tp"),
    )
    return jax.shard_map(shards, mesh=mesh, in_specs=in_specs, out_specs=out_specs, check_vma=False)
```

profile of v0, /device:TPU:0, one launch (start us, length us, event | category | flops | bytes accessed | tf_op | source)
XLA Modules:
  0.0 198.5 jit_solution(4977490238628618403)
XLA Ops:
  10.3 1.4 scatter_custom_fusion.1
  13.6 2.0 gather_fusion.2
  15.5 2.0 gather_fusion.3
  17.7 21.7 %all_to_all.58 = bf16[8,64,512]{2,1,0:T(8,128)(2,1)} all-to-all(bf16[8,64,512]{2,1,0:T(8,128)(2,1)S(1)} %bitcast.120), channel_id=1, replica_groups=mesh['ep'=8,'tp'=4] {'ep'}, dimensions={0} | all-to-all | bytes 1048576 | tf_op jit(solution)/shard_map/all_to_all | solution.py:46
  39.5 17.8 %all_to_all.59 = bf16[8,64,512]{2,1,0:T(8,128)(2,1)} all-to-all(bf16[8,64,512]{2,1,0:T(8,128)(2,1)S(1)} %bitcast.119), channel_id=1, replica_groups=mesh['ep'=8,'tp'=4] {'ep'}, dimensions={0} | all-to-all | bytes 1048576 | tf_op jit(solution)/shard_map/all_to_all | solution.py:47
  57.6 2.2 %scatter_custom_fusion = bf16[512]{0:T(512)(128)(2,1)S(1)} fusion(s32[256]{0:T(256)S(1)} %bitcast.130, bf16[256]{0:T(256)(128)(2,1)S(1)} %reshape.210, bf16[]{:T(256)} %constant.23.clone.1), kind=kCustom, calls=%fused_computation.63 | custom fusion | bytes 1026 | tf_op jit(solution)/shard_map/scatter | solution.py:38
  59.9 9.9 %all_to_all.60 = bf16[8,64,1]{1,2,0:T(2,128)(2,1)S(1)} all-to-all(bf16[8,64,1]{1,2,0:T(2,128)(2,1)S(1)} %all_to_all.52), channel_id=1, replica_groups=mesh['ep'=8,'tp'=4] {'ep'}, dimensions={0} | all-to-all | bytes 2048 | tf_op jit(solution)/shard_map/all_to_all | solution.py:48
  69.8 2.8 %convolution_bitcast_fusion.3 = f32[8,1,64,128]{3,2,0,1:T(8,128)S(1)} fusion(bf16[8,64,2048]{2,1,0:T(8,128)(2,1)} %bitcast.115, bf16[1,2048,128]{2,1,0:T(8,128)(2,1)S(1)} %copy-done), kind=kOutput, calls=%fused_computation.19 | convolution fusion | flops 268435456 | bytes 2883584 | tf_op jit(solution)/shard_map/secd,edf->secf/dot_general | solution.py:57
  72.6 1.4 convolution_bitcast_fusion.4
  74.0 11.3 %all-gather.3.cloned.1.call-done = bf16[512,2048]{1,0:T(8,128)(2,1)} async-done(((bf16[512,512]{1,0:T(8,128)(2,1)}), bf16[512,2048]{1,0:T(8,128)(2,1)}) %all-gather.3.cloned.1.call-update) | async-done | bytes 2097168 | tf_op jit(solution)/shard_map/all_gather | solution.py:52
  85.3 3.1 %multiply_reduce_fusion = (f32[8,64]{1,0:T(8,128)S(1)}, bf16[8,1,64,128]{3,2,0,1:T(8,128)(2,1)}, bf16[8,1,64,128]{3,2,0,1:T(8,128)(2,1)S(1)}, bf16[8,64,128]{2,1,0:T(8,128)(2,1)S(1)}) fusion(f32[8,1,64,128]{3,2,0,1:T(8,128)} %convolution_bitcast_fusion.4, f32[8,1,64,128]{3,2,0,1:T(8,128)S(1)} %convolution_bitcast_fusion.3, f32[8,64]{1,0:T(8,128)S(1)} %bitcast.126, ...), kind=kOutput, calls=%fused_computation.31 | convolution fusion | flops 269680128 | bytes 3543040 | tf_op jit(solution)/shard_map/secd,efd->secf/dot_general | solution.py:61
  89.2 2.0 %fusion = bf16[8,1,64,2048]{3,2,0,1:T(8,128)(2,1)} fusion(f32[8,64,2048]{2,1,0:T(8,128)S(1)} %fusion.8, bf16[8,64,128]{2,1,0:T(8,128)(2,1)S(1)} %get-tuple-element.32, bf16[1,2048,128]{2,1,0:T(8,128)(2,1)S(1)} %copy-done.3), kind=kOutput, calls=%fused_computation.8 | convolution fusion | flops 270532608 | bytes 6946816 | tf_op jit(solution)/shard_map/secf,edf->secd/dot_general | solution.py:80
  93.6 5.9 %psum.7 = bf16[8,1,64]{2,0,1:T(8,128)(2,1)S(1)} all-reduce(f32[8,1,64]{2,0,1:T(8,128)S(1)} %bitcast.132), channel_id=1, replica_groups=mesh['ep'=8,'tp'=4] {'tp'}, use_global_device_ids=true, to_apply=%region_8.10 | all-reduce | flops 512 | bytes 3072 | tf_op jit(solution)/shard_map/psum | solution.py:83
  99.5 12.0 %all_to_all.61 = bf16[8,64,1]{1,2,0:T(2,128)(2,1)S(1)} all-to-all(bf16[8,64,1]{1,2,0:T(2,128)(2,1)S(1)} %copy.31), channel_id=1, replica_groups=mesh['ep'=8,'tp'=4] {'ep'}, dimensions={0} | all-to-all | bytes 2048 | tf_op jit(solution)/shard_map/all_to_all | solution.py:91
  111.4 11.1 %reduce-scatter.3.cloned.1.call-done = bf16[8,1,64,512]{3,2,0,1:T(8,128)(2,1)} async-done(((bf16[8,1,64,2048]{3,2,0,1:T(8,128)(2,1)}), bf16[8,1,64,512]{3,2,0,1:T(8,128)(2,1)}) %reduce-scatter.3.cloned.1.call-update) | async-done | bytes 524304 | tf_op jit(solution)/shard_map/reduce_scatter | solution.py:84
  122.6 5.5 %all-to-all-start.3 = ((bf16[8,64,512]{2,1,0:T(8,128)(2,1)}), bf16[8,64,512]{2,1,0:T(8,128)(2,1)S(1)}, u32[]{:S(2)}, u32[]{:S(2)}) async-start(bf16[8,64,512]{2,1,0:T(8,128)(2,1)} %bitcast.125), calls=%async_computation.4 | async-start | bytes 1048576 | tf_op jit(solution)/shard_map/all_to_all | solution.py:88
  128.1 2.1 %convolution_convert_fusion = bf16[128,128]{1,0:T(8,128)(2,1)} fusion(bf16[128,2048]{1,0:T(8,128)(2,1)} %param.12, bf16[2048,128]{1,0:T(8,128)(2,1)} %param.18), kind=kOutput, calls=%fused_computation.22 | convolution fusion | flops 67125248 | bytes 1081344 | tf_op jit(solution)/shard_map/dot_general | solution.py:102
  130.2 3.0 %fusion.4 = bf16[1,128,2048]{2,1,0:T(8,128)(2,1)} fusion(bf16[8,64,2048]{2,1,0:T(8,128)(2,1)} %bitcast.122, f32[8,64]{1,0:T(8,128)S(1)} %bitcast.127, bf16[8,1,64,128]{3,2,0,1:T(8,128)(2,1)S(1)} %copy-done.6), kind=kOutput, calls=%fused_computation.15 | convolution fusion | flops 271843328 | bytes 2754560 | tf_op jit(solution)/shard_map/secf,secd->efd/dot_general | solution.py:68
  133.2 1.6 fusion.6
  134.8 1.6 fusion.5
  136.5 1.9 gather_fusion.1
  139.2 7.2 %all-to-all-done.3 = bf16[8,64,512]{2,1,0:T(8,128)(2,1)S(1)} async-done(((bf16[8,64,512]{2,1,0:T(8,128)(2,1)}), bf16[8,64,512]{2,1,0:T(8,128)(2,1)S(1)}, u32[]{:S(2)}, u32[]{:S(2)}) %all-to-all-start.3) | async-done | bytes 524320 | tf_op jit(solution)/shard_map/all_to_all | solution.py:88
  147.6 1.3 reduce_sum.36
  148.9 43.0 %reduce-scatter.5.cloned.1.call-done = f32[256,128]{1,0:T(8,128)} async-done(((f32[2048,128]{1,0:T(8,128)}), f32[256,128]{1,0:T(8,128)}) %reduce-scatter.5.cloned.1.call-update) | async-done | bytes 131088 | tf_op jit(solution)/shard_map/reduce_scatter | solution.py:105
  (62 shorter events, 10.8 us)
Async XLA Ops:
  7.2 62.7 %copy-start = (bf16[1,2048,128]{2,1,0:T(8,128)(2,1)S(1)}, bf16[1,2048,128]{2,1,0:T(8,128)(2,1)}, u32[]{:S(2)}) copy-start(bf16[1,2048,128]{2,1,0:T(8,128)(2,1)} %param.15) | copy-start | bytes 1572868
  7.2 62.6 %all-gather.5.cloned.1.call-start = ((), (), s32[]{:S(2)}) async-start(), calls=%async_computation.8 | async-start | bytes 2621440 | tf_op jit(solution)/shard_map/all_gather | solution.py:51
  17.7 39.7 %copy-start.8 = (f32[128,2]{0,1:T(2,128)S(1)}, f32[128,2]{0,1:T(2,128)}, u32[]{:S(2)}) copy-start(f32[128,2]{0,1:T(2,128)} %param.13) | copy-start | bytes 3076
  39.4 45.9 %all-gather.3.cloned.1.call-start = ((), (), s32[]{:S(2)}) async-start(), calls=%async_computation.7 | async-start | bytes 2621440 | tf_op jit(solution)/shard_map/all_gather | solution.py:52
  39.5 33.1 %copy-start.3 = (bf16[1,2048,128]{2,1,0:T(8,128)(2,1)S(1)}, bf16[1,2048,128]{2,1,0:T(8,128)(2,1)}, u32[]{:S(2)}) copy-start(bf16[1,2048,128]{2,1,0:T(8,128)(2,1)} %param.16) | copy-start | bytes 1572868
  57.3 65.3 %reduce-scatter.3.cloned.1.call-start = ((), (), s32[]{:S(2)}) async-start(), calls=%async_computation.9 | async-start | bytes 2621440 | tf_op jit(solution)/shard_map/reduce_scatter | solution.py:84
  69.8 2.8 %copy-start.1 = (bf16[512,2048]{1,0:T(8,128)(2,1)S(1)}, bf16[512,2048]{1,0:T(8,128)(2,1)}, u32[]{:S(2)}) copy-start(bf16[512,2048]{1,0:T(8,128)(2,1)} %all-gather.5.cloned.1.call-done) | copy-start | bytes 6291460
  88.5 0.7 copy-start.4
  91.2 1.0 copy-start.2
  91.2 1.0 copy-start.7
  91.2 39.0 %copy-start.6 = (bf16[8,1,64,128]{3,2,0,1:T(8,128)(2,1)S(1)}, bf16[8,1,64,128]{3,2,0,1:T(8,128)(2,1)}, u32[]{:S(2)}) copy-start(bf16[8,1,64,128]{3,2,0,1:T(8,128)(2,1)} %get-tuple-element.30) | copy-start | bytes 393220
  91.2 100.7 %reduce-scatter.5.cloned.1.call-start = ((), (), s32[]{:S(2)}) async-start(), calls=%async_computation.10 | async-start | bytes 1179648 | tf_op jit(solution)/shard_map/reduce_scatter | solution.py:105
  122.6 23.8 %all-to-all-start.3 = ((bf16[8,64,512]{2,1,0:T(8,128)(2,1)}), bf16[8,64,512]{2,1,0:T(8,128)(2,1)S(1)}, u32[]{:S(2)}, u32[]{:S(2)}) async-start(bf16[8,64,512]{2,1,0:T(8,128)(2,1)} %bitcast.125), calls=%async_computation.4 | async-start | bytes 1048576 | tf_op jit(solution)/shard_map/all_to_all | solution.py:88
  128.1 5.2 %copy-start.5 = (bf16[8,1,64,128]{3,2,0,1:T(8,128)(2,1)S(1)}, bf16[8,1,64,128]{3,2,0,1:T(8,128)(2,1)}, u32[]{:S(2)}) copy-start(bf16[8,1,64,128]{3,2,0,1:T(8,128)(2,1)} %copy-done.4) | copy-start | bytes 393220
Sparse Core Ops, SparseCore 0:
  39.6 21.5 all-gather.4
  62.7 22.5 all-gather.2
  91.3 31.1 reduce-scatter.2
  126.4 65.4 reduce-scatter.4
where the time goes:
time: 199 us; the launch traced here: 198 us
  waiting for transfers between devices  72.6 us (36%)
  blocking collectives  67.3 us (34%)
  matrix products  19.6 us (10%)
  local copies, waits for them, and re-layouts  16.3 us (8%)
  between operations  14 us (7%)
  starting transfers between devices  5.68 us (3%)
  other arithmetic  2.98 us (1%)
    reduce_scatter x1, waiting for transfers between devices, shards(): lax.psum_scatter(jnp.einsum('td,th->dh', cotangent, shared_hidden, prefer...  43 us
    all_to_all x1, blocking collectives, shards(): lax.all_to_all(sent_rows, 'ep', split_axis=0, concat_axis=0, tiled=True)  21.7 us
    all_to_all x1, blocking collectives, shards(): lax.all_to_all(sent_grads, 'ep', split_axis=0, concat_axis=0, tiled=True)  17.8 us
    all_to_all x1, blocking collectives, shards(): lax.all_to_all(gate_whole.astype(jnp.bfloat16).reshape(filled), 'ep', spl...  12 us
    all_gather x1, waiting for transfers between devices, shards(): lax.all_gather(got_grads, 'tp', axis=1, tiled=True)  11.3 us
    reduce_scatter x1, waiting for transfers between devices, shards(): lax.psum_scatter(partial_value.astype(jnp.bfloat16), 'tp', scatter_dimens...  11.1 us
    all_to_all x1, blocking collectives, shards(): lax.all_to_all(sent_weights, 'ep', split_axis=0, concat_axis=0, tiled=True)  9.92 us
    all_to_all x1, waiting for transfers between devices, shards(): lax.all_to_all(input_cols.reshape(filled, quarter), 'ep', split_axis=0, c...  7.17 us
  transfers between devices with their start and end apart: 5, of which 4 were waited for; matrix products, arithmetic and copies ran while one was open for 11% of the time, Pallas kernels for 0%

commit v1 on v0

--- a/solution.py
+++ b/solution.py
@@ -1,7 +1,15 @@
+import functools
 import jax
 import jax.numpy as jnp
 from jax import lax
 from jax.sharding import PartitionSpec as P
+
+
+def regions_supply_all(values, device_axis):
+    return jnp.concatenate(lax.all_gather(values, device_axis), axis=1)
+
+
+_carry_slot = functools.partial(regions_supply_all, device_axis="tp")
 
 
 def shards(
@@ -49,7 +57,7 @@
     )
     got_rows, got_grads = (
         lax.all_gather(got_rows, "tp", axis=1, tiled=True),
-        lax.all_gather(got_grads, "tp", axis=1, tiled=True),
+        _carry_slot(got_grads),
     )
     slot_rows = got_rows.reshape(ep_size, exp_local, capacity, feat_width)
     slot_grads = got_grads.reshape(ep_size, exp_local, capacity, feat_width)

time: 199 us -> 201 us (1.010)
  local copies, waits for them, and re-layouts: 16.3 us -> 23.6 us
  matrix products: 19.6 us -> 17 us
  waiting for transfers between devices: 72.6 us -> 70 us
    all_gather x1, waiting for transfers between devices: 11.3 us -> 0.01 us  [regions_supply_all(): return jnp.concatenate(lax.all_gather(values, device_axis), axis=1)]
    all_gather x1, waiting for transfers between devices: 0.01 us -> 9.29 us  [shards(): lax.all_gather(got_rows, 'tp', axis=1, tiled=True)]
    all_to_all x1, blocking collectives: 21.7 us -> 17.6 us  [shards(): lax.all_to_all(sent_rows, 'ep', split_axis=0, concat_axis=0, tiled=True)]
    all_to_all x1, blocking collectives: 17.8 us -> 21.7 us  [shards(): lax.all_to_all(sent_grads, 'ep', split_axis=0, concat_axis=0, tiled=True)]
    reshape x0 -> x1, local copies, waits for them, and re-layouts: none -> 3.54 us  [regions_supply_all(): return jnp.concatenate(lax.all_gather(values, device_axis), axis=1)]
    another operation x1 -> x2, local copies, waits for them, and re-layouts: 0.01 us -> 2.81 us
    dot_general x1, matrix products: 3.13 us -> 0.8 us  [shards(): jnp.einsum('secd,efd->secf', slot_grads, down_proj, preferred_element_typ...]
  transfers between devices with their start and end apart: 5 -> 5, of which waited for: 4 -> 4; matrix products, arithmetic and copies ran while one was open for 11% -> 12% of each run, Pallas kernels for 0% -> 0%
where the time goes in v1:
time: 201 us; the launch traced here: 200 us
  waiting for transfers between devices  70 us (35%)
  blocking collectives  67.1 us (33%)
  local copies, waits for them, and re-layouts  23.6 us (12%)
  matrix products  17 us (8%)
  between operations  14 us (7%)
  starting transfers between devices  5.68 us (3%)
  other arithmetic  2.98 us (1%)
    reduce_scatter x1, waiting for transfers between devices, shards(): lax.psum_scatter(jnp.einsum('td,th->dh', cotangent, shared_hidden, prefer...  42.9 us
    all_to_all x1, blocking collectives, shards(): lax.all_to_all(sent_grads, 'ep', split_axis=0, concat_axis=0, tiled=True)  21.7 us
    all_to_all x1, blocking collectives, shards(): lax.all_to_all(sent_rows, 'ep', split_axis=0, concat_axis=0, tiled=True)  17.6 us
    all_to_all x1, blocking collectives, shards(): lax.all_to_all(gate_whole.astype(jnp.bfloat16).reshape(filled), 'ep', spl...  12 us
    reduce_scatter x1, waiting for transfers between devices, shards(): lax.psum_scatter(partial_value.astype(jnp.bfloat16), 'tp', scatter_dimens...  10.4 us
    all_to_all x1, blocking collectives, shards(): lax.all_to_all(sent_weights, 'ep', split_axis=0, concat_axis=0, tiled=True)  9.92 us
    all_gather x1, waiting for transfers between devices, shards(): lax.all_gather(got_rows, 'tp', axis=1, tiled=True)  9.29 us
    all_to_all x1, waiting for transfers between devices, shards(): lax.all_to_all(input_cols.reshape(filled, quarter), 'ep', split_axis=0, c...  7.31 us
  transfers between devices with their start and end apart: 5, of which 4 were waited for; matrix products, arithmetic and copies ran while one was open for 12% of the time, Pallas kernels for 0%

profile of v1, /device:TPU:0, one launch (start us, length us, event | category | flops | bytes accessed | tf_op | source)
XLA Modules:
  0.0 200.3 jit_solution(3969692730079740952)
XLA Ops:
  10.3 1.4 scatter_custom_fusion.1
  13.6 2.0 gather_fusion.2
  15.5 2.0 gather_fusion.3
  17.7 21.7 %all_to_all.55 = bf16[8,64,512]{2,1,0:T(8,128)(2,1)} all-to-all(bf16[8,64,512]{2,1,0:T(8,128)(2,1)S(1)} %bitcast.120), channel_id=1, replica_groups=mesh['ep'=8,'tp'=4] {'ep'}, dimensions={0} | all-to-all | bytes 1048576 | tf_op jit(solution)/shard_map/all_to_all | solution.py:55
  39.5 17.6 %all_to_all.56 = bf16[8,64,512]{2,1,0:T(8,128)(2,1)} all-to-all(bf16[8,64,512]{2,1,0:T(8,128)(2,1)S(1)} %bitcast.119), channel_id=1, replica_groups=mesh['ep'=8,'tp'=4] {'ep'}, dimensions={0} | all-to-all | bytes 1048576 | tf_op jit(solution)/shard_map/all_to_all | solution.py:54
  57.5 2.2 %scatter_custom_fusion = bf16[512]{0:T(512)(128)(2,1)S(1)} fusion(s32[256]{0:T(256)S(1)} %bitcast.129, bf16[256]{0:T(256)(128)(2,1)S(1)} %reshape.214, bf16[]{:T(256)} %constant.23.clone.1), kind=kCustom, calls=%fused_computation.63 | custom fusion | bytes 1026 | tf_op jit(solution)/shard_map/scatter | solution.py:46
  59.8 9.9 %all_to_all.57 = bf16[8,64,1]{1,2,0:T(2,128)(2,1)S(1)} all-to-all(bf16[8,64,1]{1,2,0:T(2,128)(2,1)S(1)} %all_to_all.49), channel_id=1, replica_groups=mesh['ep'=8,'tp'=4] {'ep'}, dimensions={0} | all-to-all | bytes 2048 | tf_op jit(solution)/shard_map/all_to_all | solution.py:56
  69.7 3.5 %copy.33 = bf16[512,4,512]{2,1,0:T(4,128)(2,1)S(1)} copy(bf16[512,4,512]{2,0,1:T(8,128)(2,1)} %bitcast.121) | data formatting | bytes 4194304 | tf_op jit(solution)/shard_map/reshape | solution.py:9
  73.2 2.8 %reshape.167 = bf16[8,64,2048]{2,1,0:T(8,128)(2,1)} reshape(bf16[512,4,512]{2,1,0:T(4,128)(2,1)S(1)} %copy.33) | data formatting | bytes 4194304 | tf_op jit(solution)/shard_map/reshape.6
  76.0 9.3 %all-gather.5.cloned.1.call-done = bf16[512,2048]{1,0:T(8,128)(2,1)} async-done(((bf16[512,512]{1,0:T(8,128)(2,1)}), bf16[512,2048]{1,0:T(8,128)(2,1)}) %all-gather.5.cloned.1.call-update) | async-done | bytes 2097168 | tf_op jit(solution)/shard_map/all_gather | solution.py:59
  85.3 2.4 %convolution_bitcast_fusion.3 = f32[8,1,64,128]{3,2,0,1:T(8,128)S(1)} fusion(bf16[8,64,2048]{2,1,0:T(8,128)(2,1)} %bitcast.115, bf16[1,2048,128]{2,1,0:T(8,128)(2,1)S(1)} %copy-done), kind=kOutput, calls=%fused_computation.19 | convolution fusion | flops 268435456 | bytes 2883584 | tf_op jit(solution)/shard_map/secd,edf->secf/dot_general | solution.py:65
  91.0 2.0 %fusion = bf16[8,1,64,2048]{3,2,0,1:T(8,128)(2,1)} fusion(f32[8,64,2048]{2,1,0:T(8,128)S(1)} %fusion.8, bf16[8,64,128]{2,1,0:T(8,128)(2,1)S(1)} %get-tuple-element.32, bf16[1,2048,128]{2,1,0:T(8,128)(2,1)S(1)} %copy-done.4), kind=kOutput, calls=%fused_computation.8 | convolution fusion | flops 270532608 | bytes 6946816 | tf_op jit(solution)/shard_map/secf,edf->secd/dot_general | solution.py:88
  94.0 2.1 %fusion.28 = f32[2048,128]{1,0:T(8,128)} fusion(bf16[128,2048]{1,0:T(8,128)(2,1)S(1)} %copy-done.3, bf16[128,128]{1,0:T(8,128)(2,1)} %param.19), kind=kOutput, calls=%fused_computation.65 | convolution fusion | flops 67108864 | bytes 1605632 | tf_op jit(solution)/shard_map/td,th->dh/dot_general | solution.py:114
  96.1 5.9 %psum.7 = bf16[8,1,64]{2,0,1:T(8,128)(2,1)S(1)} all-reduce(f32[8,1,64]{2,0,1:T(8,128)S(1)} %bitcast.131), channel_id=1, replica_groups=mesh['ep'=8,'tp'=4] {'tp'}, use_global_device_ids=true, to_apply=%region_8.10 | all-reduce | flops 512 | bytes 3072 | tf_op jit(solution)/shard_map/psum | solution.py:91
  102.0 12.0 %all_to_all.58 = bf16[8,64,1]{1,2,0:T(2,128)(2,1)S(1)} all-to-all(bf16[8,64,1]{1,2,0:T(2,128)(2,1)S(1)} %copy.34), channel_id=1, replica_groups=mesh['ep'=8,'tp'=4] {'ep'}, dimensions={0} | all-to-all | bytes 2048 | tf_op jit(solution)/shard_map/all_to_all | solution.py:99
  114.0 10.4 %reduce-scatter.3.cloned.1.call-done = bf16[8,1,64,512]{3,2,0,1:T(8,128)(2,1)} async-done(((bf16[8,1,64,2048]{3,2,0,1:T(8,128)(2,1)}), bf16[8,1,64,512]{3,2,0,1:T(8,128)(2,1)}) %reduce-scatter.3.cloned.1.call-update) | async-done | bytes 524304 | tf_op jit(solution)/shard_map/reduce_scatter | solution.py:92
  124.4 5.5 %all-to-all-start.3 = ((bf16[8,64,512]{2,1,0:T(8,128)(2,1)}), bf16[8,64,512]{2,1,0:T(8,128)(2,1)S(1)}, u32[]{:S(2)}, u32[]{:S(2)}) async-start(bf16[8,64,512]{2,1,0:T(8,128)(2,1)} %bitcast.124), calls=%async_computation.4 | async-start | bytes 1048576 | tf_op jit(solution)/shard_map/all_to_all | solution.py:96
  129.9 2.1 %convolution_convert_fusion = bf16[128,128]{1,0:T(8,128)(2,1)} fusion(bf16[128,2048]{1,0:T(8,128)(2,1)} %param.12, bf16[2048,128]{1,0:T(8,128)(2,1)} %param.18), kind=kOutput, calls=%fused_computation.22 | convolution fusion | flops 67125248 | bytes 1081344 | tf_op jit(solution)/shard_map/dot_general | solution.py:110
  132.0 3.0 %fusion.4 = bf16[1,128,2048]{2,1,0:T(8,128)(2,1)} fusion(bf16[8,64,2048]{2,1,0:T(8,128)(2,1)} %reshape.167, f32[8,64]{1,0:T(8,128)S(1)} %bitcast.126, bf16[8,1,64,128]{3,2,0,1:T(8,128)(2,1)S(1)} %get-tuple-element.30), kind=kOutput, calls=%fused_computation.15 | convolution fusion | flops 271843328 | bytes 2754560 | tf_op jit(solution)/shard_map/secf,secd->efd/dot_general | solution.py:76
  135.0 1.6 fusion.6
  136.5 1.6 fusion.5
  138.2 1.9 gather_fusion.1
  140.9 7.3 %all-to-all-done.3 = bf16[8,64,512]{2,1,0:T(8,128)(2,1)S(1)} async-done(((bf16[8,64,512]{2,1,0:T(8,128)(2,1)}), bf16[8,64,512]{2,1,0:T(8,128)(2,1)S(1)}, u32[]{:S(2)}, u32[]{:S(2)}) %all-to-all-start.3) | async-done | bytes 524320 | tf_op jit(solution)/shard_map/all_to_all | solution.py:96
  150.8 42.9 %reduce-scatter.5.cloned.1.call-done = f32[256,128]{1,0:T(8,128)} async-done(((f32[2048,128]{1,0:T(8,128)}), f32[256,128]{1,0:T(8,128)}) %reduce-scatter.5.cloned.1.call-update) | async-done | bytes 131088 | tf_op jit(solution)/shard_map/reduce_scatter | solution.py:113
  (60 shorter events, 13.2 us)
Async XLA Ops:
  7.2 78.2 %copy-start = (bf16[1,2048,128]{2,1,0:T(8,128)(2,1)S(1)}, bf16[1,2048,128]{2,1,0:T(8,128)(2,1)}, u32[]{:S(2)}) copy-start(bf16[1,2048,128]{2,1,0:T(8,128)(2,1)} %param.15) | copy-start | bytes 1572868
  7.2 62.5 %all-gather.3.cloned.1.call-start = ((), (), s32[]{:S(2)}) async-start(), calls=%async_computation.7 | async-start | bytes 2621440 | tf_op jit(solution)/shard_map/all_gather | solution.py:9
  17.7 39.5 %copy-start.6 = (f32[128,2]{0,1:T(2,128)S(1)}, f32[128,2]{0,1:T(2,128)}, u32[]{:S(2)}) copy-start(f32[128,2]{0,1:T(2,128)} %param.13) | copy-start | bytes 3076
  39.4 45.9 %all-gather.5.cloned.1.call-start = ((), (), s32[]{:S(2)}) async-start(), calls=%async_computation.8 | async-start | bytes 2621440 | tf_op jit(solution)/shard_map/all_gather | solution.py:59
  57.1 67.2 %reduce-scatter.3.cloned.1.call-start = ((), (), s32[]{:S(2)}) async-start(), calls=%async_computation.9 | async-start | bytes 2621440 | tf_op jit(solution)/shard_map/reduce_scatter | solution.py:92
  76.0 11.7 %copy-start.4 = (bf16[1,2048,128]{2,1,0:T(8,128)(2,1)S(1)}, bf16[1,2048,128]{2,1,0:T(8,128)(2,1)}, u32[]{:S(2)}) copy-start(bf16[1,2048,128]{2,1,0:T(8,128)(2,1)} %param.16) | copy-start | bytes 1572868
  85.3 2.5 %copy-start.1 = (bf16[512,2048]{1,0:T(8,128)(2,1)S(1)}, bf16[512,2048]{1,0:T(8,128)(2,1)}, u32[]{:S(2)}) copy-start(bf16[512,2048]{1,0:T(8,128)(2,1)} %all-gather.5.cloned.1.call-done) | copy-start | bytes 6291460
  87.8 1.6 copy-start.2
  87.8 1.7 copy-start.5
  93.0 1.0 copy-start.3
  93.0 100.7 %reduce-scatter.5.cloned.1.call-start = ((), (), s32[]{:S(2)}) async-start(), calls=%async_computation.10 | async-start | bytes 1179648 | tf_op jit(solution)/shard_map/reduce_scatter | solution.py:113
  124.4 23.9 %all-to-all-start.3 = ((bf16[8,64,512]{2,1,0:T(8,128)(2,1)}), bf16[8,64,512]{2,1,0:T(8,128)(2,1)S(1)}, u32[]{:S(2)}, u32[]{:S(2)}) async-start(bf16[8,64,512]{2,1,0:T(8,128)(2,1)} %bitcast.124), calls=%async_computation.4 | async-start | bytes 1048576 | tf_op jit(solution)/shard_map/all_to_all | solution.py:96
Sparse Core Ops, SparseCore 0:
  39.6 21.5 all-gather.2
  62.7 22.5 all-gather.4
  93.2 31.1 reduce-scatter.2
  128.2 65.5 reduce-scatter.4
